TPU v7x, 32 devices: a whole 2x2x4 slice. The times are simulated.
32 devices in a mesh: ra: 4 (over z), cb: 4 (over y, x), dp: 2 (over core).
Axes of the slice: x: 2, y: 2, z: 4, core: 2. Of those that a mesh axis runs over, the one named last changes fastest.
Arguments:
- tokens: bfloat16 [128, 4096], P('dp', 'ra'), may hold values from -45 to 45
- gain_first: bfloat16 [4096], P('ra'), may hold values from 0.099609375 to 1.8984375
- up_first: float32 [4096, 16384], P('ra', 'cb'), may hold values from -0.125 to 0.125
- up_scale_first: float32 [16384], P('cb'), may hold values from 0.5 to 2
- down_first: float32 [16384, 4096], P('cb', 'ra'), may hold values from -0.046875 to 0.046875
- down_scale_first: float32 [4096], P('ra'), may hold values from 0.5 to 2
- gain_second: bfloat16 [4096], P('ra'), may hold values from 0.099609375 to 1.8984375
- up_second: float32 [4096, 16384], P('ra', 'cb'), may hold values from -0.125 to 0.125
- up_scale_second: float32 [16384], P('cb'), may hold values from 0.5 to 2
- down_second: float32 [16384, 4096], P('cb', 'ra'), may hold values from -0.046875 to 0.046875
- down_scale_second: float32 [4096], P('ra'), may hold values from 0.5 to 2
Outputs:
- mixed_out: bfloat16 [128, 4096], P('dp', 'ra')
All inputs are finite; a program needn't handle non-finite values.
Results may differ from a plain program's by a relative error of at most 0.02.
Values may be sent and summed in bfloat16 or wider, within the bound.
A program may use at most 128 MiB of HBM per device.

v0:
```python
import jax
import jax.numpy as jnp
from jax import lax
from jax.sharding import PartitionSpec as P

epsilon = 1e-06
residual_share = 0.25


def sub_layer(inputs, norm_gain, up_weight, up_scale, down_weight, down_scale):
    values = inputs.astype(jnp.float32)
    full_width = inputs.shape[1] * lax.axis_size("ra")
    squares = lax.psum(jnp.sum(values * values, axis=1, keepdims=True), "ra")
    inverse = lax.rsqrt(squares / full_width + epsilon)
    normed = (values * inverse * norm_gain.astype(jnp.float32)).astype(jnp.bfloat16)
    partial_value = jnp.dot(
        normed, up_weight.astype(jnp.bfloat16), preferred_element_type=jnp.float32
    )
    shares = lax.psum_scatter(partial_value, "ra", scatter_dimension=1, tiled=True)
    share_width = shares.shape[1]
    own_scale = lax.dynamic_slice_in_dim(
        up_scale, lax.axis_index("ra") * share_width, share_width, 0
    )
    own_units = jnp.square(jax.nn.relu(shares * own_scale)).astype(jnp.bfloat16)
    hidden = lax.all_gather(own_units, "ra", axis=1, tiled=True)
    projected = jnp.dot(
        hidden, down_weight.astype(jnp.bfloat16), preferred_element_type=jnp.float32
    ).astype(jnp.bfloat16)
    projected = lax.optimization_barrier(projected).astype(jnp.float32)
    total = lax.psum(projected.astype(jnp.bfloat16), "cb").astype(jnp.float32)
    return (residual_share * values + total * down_scale).astype(jnp.bfloat16)


def shards(
    tokens,
    gain_first,
    up_first,
    up_scale_first,
    down_first,
    down_scale_first,
    gain_second,
    up_second,
    up_scale_second,
    down_second,
    down_scale_second,
):
    carried = sub_layer(tokens, gain_first, up_first, up_scale_first, down_first, down_scale_first)
    return sub_layer(
        carried, gain_second, up_second, up_scale_second, down_second, down_scale_second
    )


def solution(mesh):
    in_specs = (
        P("dp", "ra"),
        P("ra"),
        P("ra", "cb"),
        P("cb"),
        P("cb", "ra"),
        P("ra"),
        P("ra"),
        P("ra", "cb"),
        P("cb"),
        P("cb", "ra"),
        P("ra"),
    )
    out_specs = P("dp", "ra")
    return jax.shard_map(shards, mesh=mesh, in_specs=in_specs, out_specs=out_specs, check_vma=False)
```

profile of v0, /device:TPU:0, one launch (start us, length us, event | category | flops | bytes accessed | tf_op | source)
XLA Modules:
  0.0 241.5 jit_solution(8065290762153675405)
XLA Ops:
  6.5 0.0 reduce-scatter.3.cloned.1.call-start
  6.5 0.7 convert_element_type.59
  7.2 1.0 fusion.16
  8.3 13.5 %psum.28 = f32[64,1]{0,1:T(1,128)S(1)} all-reduce(f32[64,1]{0,1:T(1,128)S(1)} %bitcast.9), channel_id=1, replica_groups=mesh['ra'=4,'cb'=4,'dp'=2] {'ra'}, use_global_device_ids=true, to_apply=%region_1.0 | all-reduce | flops 64 | bytes 512 | tf_op jit(solution)/shard_map/psum | solution.py:13
  21.8 0.0 copy-start.3
  21.8 0.0 copy-start
  21.8 0.0 copy-start.1
  21.8 8.5 %fusion.6 = f32[64,4096]{1,0:T(8,128)} fusion(f32[1024,4096]{1,0:T(8,128)} %param.13, bf16[64,1024]{1,0:T(8,128)(2,1)} %param.11, f32[1024]{0:T(1024)S(1)} %convert_element_type.59, f32[64]{0:T(128)S(1)} %rsqrt_bitcast_fusion.1), kind=kOutput, calls=%fused_computation.6 | convolution fusion | flops 541327360 | bytes 17961216 | tf_op jit(solution)/shard_map/dot_general | solution.py:16
  30.3 0.0 reduce-scatter.3.cloned.1.call-update
  30.3 0.0 all-reduce.3.cloned.1.call-start
  30.4 0.7 dynamic_slice.6
  31.1 24.9 %reduce-scatter.3.cloned.1.call-done = f32[64,1024]{1,0:T(8,128)} async-done(((f32[64,4096]{1,0:T(8,128)}), f32[64,1024]{1,0:T(8,128)}) %reduce-scatter.3.cloned.1.call-update) | async-done | bytes 262160 | tf_op jit(solution)/shard_map/reduce_scatter | solution.py:19
  56.0 1.0 multiply_convert_fusion.1
  56.9 16.0 %all_gather.6 = bf16[64,4096]{1,0:T(8,128)(2,1)S(1)} all-gather(bf16[64,1024]{1,0:T(8,128)(2,1)S(1)} %multiply_convert_fusion.1), channel_id=1, replica_groups=mesh['ra'=4,'cb'=4,'dp'=2] {'ra'}, dimensions={1}, use_global_device_ids=true | all-gather | bytes 655360 | tf_op jit(solution)/shard_map/all_gather | solution.py:25
  73.0 0.0 dynamic-slice-start
  73.0 8.0 %fusion.8 = bf16[64,1024]{1,0:T(8,128)(2,1)} fusion(bf16[64,4096]{1,0:T(8,128)(2,1)S(1)} %all_gather.6, f32[4096,1024]{1,0:T(8,128)} %param.15), kind=kOutput, calls=%fused_computation.8 | convolution fusion | flops 541130752 | bytes 17432576 | tf_op jit(solution)/shard_map/dot_general | solution.py:26
  81.0 0.0 all-reduce.3.cloned.1.call-update
  81.0 0.0 reduce-scatter.5.cloned.1.call-start
  81.1 0.0 copy-done.3
  81.1 40.6 %all-reduce.3.cloned.1.call-done = bf16[64,1024]{1,0:T(8,128)(2,1)} async-done(((bf16[64,1024]{1,0:T(8,128)(2,1)}), bf16[64,1024]{1,0:T(8,128)(2,1)}) %all-reduce.3.cloned.1.call-update) | async-done | bytes 131088 | tf_op jit(solution)/shard_map/psum | solution.py:30
  121.7 0.0 copy-done
  121.7 0.0 copy-done.1
  121.7 1.1 fusion.21
  122.8 11.7 %psum.30 = f32[64,1]{0,1:T(1,128)S(1)} all-reduce(f32[64,1]{0,1:T(1,128)S(1)} %bitcast.8), channel_id=1, replica_groups=mesh['ra'=4,'cb'=4,'dp'=2] {'ra'}, use_global_device_ids=true, to_apply=%region_5.6 | all-reduce | flops 64 | bytes 512 | tf_op jit(solution)/shard_map/psum | solution.py:13
  134.5 0.0 copy-start.2
  134.5 8.4 %fusion.2 = f32[64,4096]{1,0:T(8,128)} fusion(f32[1024,4096]{1,0:T(8,128)} %param.18, bf16[64,1024]{1,0:T(8,128)(2,1)S(1)} %get-tuple-element.6, f32[1024]{0:T(1024)S(1)} %convert_element_type.68, f32[64]{0:T(128)S(1)} %rsqrt_bitcast_fusion), kind=kOutput, calls=%fused_computation.2 | convolution fusion | flops 541327360 | bytes 17961216 | tf_op jit(solution)/shard_map/dot_general | solution.py:16
  142.9 0.0 reduce-scatter.5.cloned.1.call-update
  143.0 0.0 all-reduce.5.cloned.1.call-start
  143.0 24.6 %reduce-scatter.5.cloned.1.call-done = f32[64,1024]{1,0:T(8,128)} async-done(((f32[64,4096]{1,0:T(8,128)}), f32[64,1024]{1,0:T(8,128)}) %reduce-scatter.5.cloned.1.call-update) | async-done | bytes 262160 | tf_op jit(solution)/shard_map/reduce_scatter | solution.py:19
  167.6 0.0 dynamic-slice-done
  167.6 1.0 multiply_convert_fusion
  168.6 15.9 %all_gather.7 = bf16[64,4096]{1,0:T(8,128)(2,1)S(1)} all-gather(bf16[64,1024]{1,0:T(8,128)(2,1)S(1)} %multiply_convert_fusion), channel_id=1, replica_groups=mesh['ra'=4,'cb'=4,'dp'=2] {'ra'}, dimensions={1}, use_global_device_ids=true | all-gather | bytes 655360 | tf_op jit(solution)/shard_map/all_gather | solution.py:25
  184.5 8.0 %fusion.11 = bf16[64,1024]{1,0:T(8,128)(2,1)} fusion(bf16[64,4096]{1,0:T(8,128)(2,1)S(1)} %all_gather.7, f32[4096,1024]{1,0:T(8,128)} %param.20), kind=kOutput, calls=%fused_computation.9 | convolution fusion | flops 541130752 | bytes 17432576 | tf_op jit(solution)/shard_map/dot_general | solution.py:26
  192.6 0.0 all-reduce.5.cloned.1.call-update
  192.6 40.8 %all-reduce.5.cloned.1.call-done = bf16[64,1024]{1,0:T(8,128)(2,1)} async-done(((bf16[64,1024]{1,0:T(8,128)(2,1)}), bf16[64,1024]{1,0:T(8,128)(2,1)}) %all-reduce.5.cloned.1.call-update) | async-done | bytes 131088 | tf_op jit(solution)/shard_map/psum | solution.py:30
  233.4 0.0 copy-done.2
  233.4 1.6 fusion.20
  (3 shorter events, 0.0 us)
Async XLA Ops:
  6.5 49.4 %reduce-scatter.3.cloned.1.call-start = ((), (), s32[]{:S(2)}) async-start(), calls=%async_computation.2 | async-start | bytes 1310720 | tf_op jit(solution)/shard_map/reduce_scatter | solution.py:19
  21.8 59.3 %copy-start.3 = (bf16[1024]{0:T(1024)(128)(2,1)S(1)}, bf16[1024]{0:T(1024)(128)(2,1)}, u32[]{:S(2)}) copy-start(bf16[1024]{0:T(1024)(128)(2,1)} %param.17) | copy-start | bytes 6148
  21.8 100.0 %copy-start = (bf16[64,1024]{1,0:T(8,128)(2,1)S(1)}, bf16[64,1024]{1,0:T(8,128)(2,1)}, u32[]{:S(2)}) copy-start(bf16[64,1024]{1,0:T(8,128)(2,1)} %param.11) | copy-start | bytes 393220
  21.8 100.0 %copy-start.1 = (f32[1024]{0:T(1024)S(1)}, f32[1024]{0:T(1024)}, u32[]{:S(2)}) copy-start(f32[1024]{0:T(1024)} %param.16) | copy-start | bytes 12292
  30.3 91.4 %all-reduce.3.cloned.1.call-start = ((), (), s32[]{:S(2)}) async-start(), calls=%async_computation.3 | async-start | bytes 262144 | tf_op jit(solution)/shard_map/psum | solution.py:30
  73.0 94.7 %dynamic-slice-start = ((f32[4096]{0:T(1024)}, s32[]{:T(128)}), f32[1024]{0:T(1024)S(1)}, s32[]{:S(2)}) async-start(f32[4096]{0:T(1024)} %param.19, s32[]{:T(128)} %select_n.4), calls=%async_computation.6 | async-start | bytes 8704 | tf_op jit(solution)/shard_map/dynamic_slice | solution.py:21
  81.0 86.6 %reduce-scatter.5.cloned.1.call-start = ((), (), s32[]{:S(2)}) async-start(), calls=%async_computation.4 | async-start | bytes 1310720 | tf_op jit(solution)/shard_map/reduce_scatter | solution.py:19
  134.5 98.8 %copy-start.2 = (f32[1024]{0:T(1024)S(1)}, f32[1024]{0:T(1024)}, u32[]{:S(2)}) copy-start(f32[1024]{0:T(1024)} %param.21) | copy-start | bytes 12292
  143.0 90.4 %all-reduce.5.cloned.1.call-start = ((), (), s32[]{:S(2)}) async-start(), calls=%async_computation.5 | async-start | bytes 262144 | tf_op jit(solution)/shard_map/psum | solution.py:30
Sparse Core Ops, SparseCore 0:
  30.4 25.4 reduce-scatter.2
  81.1 40.5 all-reduce.2
  143.1 24.5 reduce-scatter.4
  192.7 40.5 all-reduce.4
where the time goes:
time: 242 us
  waiting for transfers between devices  131 us (54%)
  blocking collectives  57.1 us (24%)
  matrix products  33 us (14%)
  between operations  13.2 us (5%)
  other arithmetic  6.38 us (3%)
    psum x2, waiting for transfers between devices, sub_layer(): total = lax.psum(projected.astype(jnp.bfloat16), 'cb').astype(jnp.float32)  81.4 us
    reduce_scatter x2, waiting for transfers between devices, sub_layer(): lax.psum_scatter(partial_value, 'ra', scatter_dimension=1, tiled=True)  49.5 us
    all_gather x2, blocking collectives, sub_layer(): hidden = lax.all_gather(own_units, 'ra', axis=1, tiled=True)  31.9 us
    psum x2, blocking collectives, sub_layer(): squares = lax.psum(jnp.sum(values * values, axis=1, keepdims=True), 'ra')  25.2 us
    dot_general x2, matrix products, sub_layer(): jnp.dot(normed, up_weight.astype(jnp.bfloat16), preferred_element_type=jn...  16.9 us
    dot_general x2, matrix products, sub_layer(): jnp.dot(hidden, down_weight.astype(jnp.bfloat16), preferred_element_type=...  16.1 us
  transfers between devices with their start and end apart: 4, of which 4 were waited for; matrix products, arithmetic and copies ran while one was open for 0% of the time, Pallas kernels for 0%

commit v1 on v0

--- a/solution.py
+++ b/solution.py
@@ -1,10 +1,371 @@
+import functools
+
 import jax
 import jax.numpy as jnp
 from jax import lax
+from jax.experimental import pallas as pl
+from jax.experimental.pallas import tpu as pltpu
 from jax.sharding import PartitionSpec as P
 
 epsilon = 1e-06
 residual_share = 0.25
+MESH = pl.DeviceIdType.MESH
+LANES = 128
+VMEM_BYTES = 67043328
+
+
+def visit_order(count):
+    return sorted(range(1, count), key=lambda offset: (abs(2 * offset - count), offset))
+
+
+def fused_kernel(
+    plan,
+    tokens_ref,
+    gain_a,
+    up_scale_a,
+    down_scale_a,
+    gain_b,
+    up_scale_b,
+    down_scale_b,
+    up_a,
+    down_a,
+    up_b,
+    down_b,
+    out_ref,
+    weights,
+    scaled,
+    own_partial,
+    rs_out,
+    rs_in,
+    stat_out,
+    stat_in,
+    hidden_own,
+    hidden_in,
+    acc,
+    part,
+    cb_in,
+    fresh,
+    state,
+    w_sem,
+    rs_sem,
+    stat_sem,
+    ag_sem,
+    cb_sem,
+    cg_sem,
+):
+    n_ra, n_cb, groups, tile = plan
+    gains, up_scales, down_scales = (gain_a, gain_b), (up_scale_a, up_scale_b), (down_scale_a, down_scale_b)
+    rows_all, width = tokens_ref.shape
+    rows = rows_all // groups
+    units = hidden_own.shape[2]
+    block = width // n_cb
+    full_width = width * n_ra
+    r, c = lax.axis_index("ra"), lax.axis_index("cb")
+    ra_order, cb_order = visit_order(n_ra), visit_order(n_cb)
+    own_columns = pl.ds(pl.multiple_of(c * block, LANES), block)
+    sends = []
+
+    def up_copy(layer, j):
+        source = (up_a, up_b)[layer]
+        buffer = (0, 2)[layer]
+        start = pl.multiple_of(lax.rem(r + j, n_ra) * units, LANES)
+        return pltpu.make_async_copy(source.at[:, pl.ds(start, units)], weights.at[buffer, j], w_sem.at[2 * layer, j])
+
+    def down_copy(layer, j):
+        source = (down_a, down_b)[layer]
+        buffer = (1, 0)[layer]
+        start = pl.multiple_of(lax.rem(r + n_ra - j, n_ra) * units, LANES)
+        return pltpu.make_async_copy(source.at[pl.ds(start, units), :], weights.at[buffer, j], w_sem.at[2 * layer + 1, j])
+
+    up_order = ra_order + [0]
+    down_order = [0] + ra_order
+    queue = [up_copy(0, j) for j in up_order] + [down_copy(0, j) for j in down_order]
+    queue += [up_copy(1, j) for j in up_order]
+    issued = [0]
+
+    def issue(count):
+        for copy in queue[issued[0] : issued[0] + count]:
+            copy.start()
+        issued[0] += count
+
+    issue(2)
+
+    barrier = pltpu.get_barrier_semaphore()
+    for j in range(1, n_ra):
+        pl.semaphore_signal(barrier, inc=1, device_id={"ra": lax.rem(r + j, n_ra)}, device_id_type=MESH)
+    for j in range(1, n_cb):
+        pl.semaphore_signal(barrier, inc=1, device_id={"cb": lax.rem(c + j, n_cb)}, device_id_type=MESH)
+
+    row_ids = lax.broadcasted_iota(jnp.int32, (rows, LANES), 0)
+    lane_ids = lax.broadcasted_iota(jnp.int32, (rows, LANES), 1)
+    eye = row_ids == lane_ids
+
+    def send(axis, index, count, j, source, target, sem):
+        copy = pltpu.make_async_remote_copy(
+            src_ref=source,
+            dst_ref=target,
+            send_sem=sem.at[0],
+            recv_sem=sem.at[1],
+            device_id={axis: lax.rem(index + j, count)},
+            device_id_type=MESH,
+        )
+        copy.start()
+        sends.append(copy)
+        return copy
+
+    stat_copies, rs_copies, ag_copies, cb_copies, cg_copies = {}, {}, {}, {}, {}
+    waited = set()
+
+    def span(g):
+        return pl.ds(g * rows, rows)
+
+    def prepare(layer, g):
+        values = (tokens_ref[span(g), :] if layer == 0 else state[0, span(g), :]).astype(jnp.float32)
+        squares = jnp.sum(values * values, axis=1, keepdims=True)
+        as_row = jnp.sum(jnp.where(eye, squares, 0.0), axis=0, keepdims=True)
+        stat_out[layer, g] = jnp.broadcast_to(as_row, (8, LANES))
+        scaled[layer, span(g), :] = (values * gains[layer][...].astype(jnp.float32)).astype(jnp.bfloat16)
+
+    def send_stats(layer, g):
+        for j in ra_order:
+            stat_copies[layer, g, j] = send(
+                "ra", r, n_ra, j, stat_out.at[layer, g], stat_in.at[layer, g, j - 1], stat_sem.at[layer, g, j - 1]
+            )
+
+    def wait_weight(kind, layer, j):
+        if (kind, layer, j) not in waited:
+            waited.add((kind, layer, j))
+            (up_copy if kind == "up" else down_copy)(layer, j).wait()
+            if kind == "up" and layer == 0:
+                issue(1)
+
+    def up_stage(layer, members):
+        low, count = members[0] * rows, len(members) * rows
+        buffer = (0, 2)[layer]
+        for j in up_order:
+            wait_weight("up", layer, j)
+
+            def body(i, carry):
+                columns = pl.ds(pl.multiple_of(i * tile, LANES), tile)
+                value = jnp.dot(
+                    scaled[layer, pl.ds(low, count), :],
+                    weights[buffer, j, :, columns].astype(jnp.bfloat16),
+                    preferred_element_type=jnp.float32,
+                )
+                if j == 0:
+                    own_partial[pl.ds(low, count), columns] = value
+                else:
+                    rs_out[layer, j - 1, pl.ds(low, count), columns] = value.astype(jnp.bfloat16)
+                return carry
+
+            lax.fori_loop(0, units // tile, body, 0)
+            if j:
+                for g in members:
+                    rs_copies[layer, g, j] = send(
+                        "ra",
+                        r,
+                        n_ra,
+                        j,
+                        rs_out.at[layer, j - 1, span(g), :],
+                        rs_in.at[layer, j - 1, span(g), :],
+                        rs_sem.at[layer, g, j - 1],
+                    )
+
+    def reduce_stage(layer, g):
+        total = own_partial[span(g), :]
+        squares = stat_out[layer, g]
+        for j in ra_order:
+            stat_copies[layer, g, j].wait_recv()
+            squares = squares + stat_in[layer, g, j - 1]
+        as_column = jnp.sum(jnp.where(eye, jnp.broadcast_to(squares[0:1, :], (rows, LANES)), 0.0), axis=1, keepdims=True)
+        inverse = lax.rsqrt(as_column / full_width + epsilon)
+        for j in ra_order:
+            rs_copies[layer, g, j].wait_recv()
+            total = total + rs_in[layer, j - 1, span(g), :].astype(jnp.float32)
+        scale = up_scales[layer][:, pl.ds(pl.multiple_of(r * units, LANES), units)]
+        active = jnp.square(jnp.maximum(total * inverse * scale, 0.0))
+        hidden_own[layer, span(g), :] = active.astype(jnp.bfloat16)
+        for j in ra_order:
+            ag_copies[layer, g, j] = send(
+                "ra",
+                r,
+                n_ra,
+                j,
+                hidden_own.at[layer, span(g), :],
+                hidden_in.at[layer, j - 1, span(g), :],
+                ag_sem.at[layer, g, j - 1],
+            )
+
+    def down_stage(layer, g):
+        buffer = (1, 0)[layer]
+        for j in down_order:
+            wait_weight("down", layer, j)
+            if j:
+                ag_copies[layer, g, j].wait_recv()
+
+            def body(i, carry):
+                columns = pl.ds(pl.multiple_of(i * tile, LANES), tile)
+                source = hidden_own[layer, span(g), :] if j == 0 else hidden_in[layer, j - 1, span(g), :]
+                value = jnp.dot(
+                    source, weights[buffer, j, :, columns].astype(jnp.bfloat16), preferred_element_type=jnp.float32
+                )
+                if j == down_order[0]:
+                    acc[:, columns] = value
+                elif j == down_order[-1]:
+                    part[layer, span(g), columns] = (acc[:, columns] + value).astype(jnp.bfloat16)
+                else:
+                    acc[:, columns] += value
+                return carry
+
+            lax.fori_loop(0, width // tile, body, 0)
+        for j in cb_order:
+            start = pl.multiple_of(lax.rem(c + j, n_cb) * block, LANES)
+            cb_copies[layer, g, j] = send(
+                "cb",
+                c,
+                n_cb,
+                j,
+                part.at[layer, span(g), pl.ds(start, block)],
+                cb_in.at[layer, j - 1, span(g), :],
+                cb_sem.at[layer, g, j - 1],
+            )
+
+    def combine_stage(layer, g):
+        total = part[layer, span(g), own_columns].astype(jnp.float32)
+        for j in cb_order:
+            cb_copies[layer, g, j].wait_recv()
+            total = total + cb_in[layer, j - 1, span(g), :].astype(jnp.float32)
+        before = (tokens_ref[span(g), own_columns] if layer == 0 else state[0, span(g), own_columns]).astype(jnp.float32)
+        after = residual_share * before + total * down_scales[layer][:, own_columns]
+        after = after.astype(jnp.bfloat16)
+        fresh[layer, span(g), :] = after
+        state[layer, span(g), own_columns] = after
+        for j in cb_order:
+            cg_copies[layer, g, j] = send(
+                "cb",
+                c,
+                n_cb,
+                j,
+                fresh.at[layer, span(g), :],
+                state.at[layer, span(g), own_columns],
+                cg_sem.at[layer, g, j - 1],
+            )
+
+    def gather_stage(layer, g):
+        for j in cb_order:
+            cg_copies[layer, g, j].wait_recv()
+        if layer == 1:
+            out_ref[span(g), :] = state[1, span(g), :]
+        else:
+            prepare(1, g)
+            send_stats(1, g)
+            up_stage(1, [g])
+
+    everyone = list(range(groups))
+    for g in everyone:
+        prepare(0, g)
+    pl.semaphore_wait(barrier, n_ra + n_cb - 2)
+    for g in everyone:
+        send_stats(0, g)
+    up_stage(0, everyone)
+    issue(len(queue))
+    for j in down_order:
+        down_copy(1, j).start()
+    for layer in range(2):
+        for g in everyone:
+            reduce_stage(layer, g)
+        for g in everyone:
+            down_stage(layer, g)
+            if g:
+                gather_stage(layer, g - 1)
+            combine_stage(layer, g)
+        gather_stage(layer, groups - 1)
+    for copy in sends:
+        copy.wait_send()
+
+
+def fused_shards(
+    plan,
+    tokens,
+    gain_first,
+    up_first,
+    up_scale_first,
+    down_first,
+    down_scale_first,
+    gain_second,
+    up_second,
+    up_scale_second,
+    down_second,
+    down_scale_second,
+):
+    n_ra, n_cb, groups, _ = plan
+    rows_all, width = tokens.shape
+    units = up_first.shape[1] // n_ra
+    block = width // n_cb
+    bf, f32 = jnp.bfloat16, jnp.float32
+    small = pl.BlockSpec(memory_space=pltpu.VMEM)
+    large = pl.BlockSpec(memory_space=pl.ANY)
+
+    def sems(count):
+        return pltpu.SemaphoreType.DMA((2, groups, count - 1, 2))
+
+    return pl.pallas_call(
+        functools.partial(fused_kernel, plan),
+        out_shape=jax.ShapeDtypeStruct(tokens.shape, tokens.dtype),
+        in_specs=[small] * 7 + [large] * 4,
+        out_specs=small,
+        scratch_shapes=[
+            pltpu.VMEM((3, n_ra, width, units), f32),
+            pltpu.VMEM((2, rows_all, width), bf),
+            pltpu.VMEM((rows_all, units), f32),
+            pltpu.VMEM((2, n_ra - 1, rows_all, units), bf),
+            pltpu.VMEM((2, n_ra - 1, rows_all, units), bf),
+            pltpu.VMEM((2, groups, 8, LANES), f32),
+            pltpu.VMEM((2, groups, n_ra - 1, 8, LANES), f32),
+            pltpu.VMEM((2, rows_all, units), bf),
+            pltpu.VMEM((2, n_ra - 1, rows_all, units), bf),
+            pltpu.VMEM((rows_all // groups, width), f32),
+            pltpu.VMEM((2, rows_all, width), bf),
+            pltpu.VMEM((2, n_cb - 1, rows_all, block), bf),
+            pltpu.VMEM((2, rows_all, block), bf),
+            pltpu.VMEM((2, rows_all, width), bf),
+            pltpu.SemaphoreType.DMA((4, n_ra)),
+            sems(n_ra),
+            sems(n_ra),
+            sems(n_ra),
+            sems(n_cb),
+            sems(n_cb),
+        ],
+        compiler_params=pltpu.CompilerParams(collective_id=0, has_side_effects=True, vmem_limit_bytes=VMEM_BYTES),
+    )(
+        tokens,
+        gain_first[None, :],
+        up_scale_first[None, :],
+        down_scale_first[None, :],
+        gain_second[None, :],
+        up_scale_second[None, :],
+        down_scale_second[None, :],
+        up_first,
+        down_first,
+        up_second,
+        down_second,
+    )
+
+
+def plan_for(mesh, d, ff, tokens):
+    n_ra, n_cb, n_dp = mesh.shape["ra"], mesh.shape["cb"], mesh.shape["dp"]
+    width, units, rows = d // n_ra, ff // (n_cb * n_ra), tokens // n_dp
+    if n_ra < 2 or n_cb < 2 or width != units or width % (n_cb * LANES) or rows % 16 or rows > LANES:
+        return None
+    if 3 * n_ra * width * units * 4 > VMEM_BYTES * 4 // 5:
+        return None
+    groups = GROUPS if rows % (16 * GROUPS) == 0 else 1
+    tile = TILE if width % TILE == 0 else LANES
+    return n_ra, n_cb, groups, tile
+
+
+GROUPS = 2
+TILE = 512
 
 
 def sub_layer(inputs, norm_gain, up_weight, up_scale, down_weight, down_scale):
@@ -65,4 +426,12 @@
         P("ra"),
     )
     out_specs = P("dp", "ra")
-    return jax.shard_map(shards, mesh=mesh, in_specs=in_specs, out_specs=out_specs, check_vma=False)
+
+    def run(*arrays):
+        tokens, up_weight = arrays[0], arrays[2]
+        plan = plan_for(mesh, up_weight.shape[0], up_weight.shape[1], tokens.shape[0])
+        inner = shards if plan is None else functools.partial(fused_shards, plan)
+        mapped = jax.shard_map(inner, mesh=mesh, in_specs=in_specs, out_specs=out_specs, check_vma=False)
+        return mapped(*arrays)
+
+    return run

time: 242 us -> 78.4 us (0.32)
  waiting for transfers between devices: 131 us -> 0 us
  Pallas kernels: 0 us -> 74.1 us
  blocking collectives: 57.1 us -> 0 us
  matrix products: 33 us -> 0 us
  between operations: 13.2 us -> 0.01 us
  other arithmetic: 6.38 us -> 0 us
  local copies, waits for them, and re-layouts: 0.71 us -> 4.12 us
    psum x2 -> x0, waiting for transfers between devices: 81.4 us -> none  [sub_layer(): total = lax.psum(projected.astype(jnp.bfloat16), 'cb').astype(jnp.float32)]
    pallas_call x0 -> x1, Pallas kernels: none -> 74.1 us  [fused_shards(): pl.pallas_call(functools.partial(fused_kernel, plan), out_shape=jax.Shape...]
    reduce_scatter x2 -> x0, waiting for transfers between devices: 49.5 us -> none  [sub_layer(): lax.psum_scatter(partial_value, 'ra', scatter_dimension=1, tiled=True)]
    dot_general x4 -> x0, matrix products: 33 us -> none  [the longest x2 16.9 us: sub_layer(): jnp.dot(normed, up_weight.astype(jnp.bfloat16), preferred_element_type=jn...]
    all_gather x2 -> x0, blocking collectives: 31.9 us -> none  [sub_layer(): hidden = lax.all_gather(own_units, 'ra', axis=1, tiled=True)]
    psum x2 -> x0, blocking collectives: 25.2 us -> none  [sub_layer(): squares = lax.psum(jnp.sum(values * values, axis=1, keepdims=True), 'ra')]
    convert_element_type x5 -> x0, other arithmetic: 4.26 us -> none  [the longest x2 1.97 us: sub_layer(): own_units = jnp.square(jax.nn.relu(shares * own_scale)).astype(jnp.bfloat16)]
    broadcast_in_dim x0 -> x2, local copies, waits for them, and re-layouts: none -> 2.55 us  [the longest x1 1.28 us: fused_shards(): gain_first[None, :]]
  transfers between devices with their start and end apart: 4 -> 0, of which waited for: 4 -> 0; matrix products, arithmetic and copies ran while one was open for 0% -> 0% of each run, Pallas kernels for 0% -> 0%
where the time goes in v1:
time: 78.4 us; the launch traced here: 78.2 us
  Pallas kernels  74.1 us (95%)
  local copies, waits for them, and re-layouts  4.12 us (5%)
    pallas_call x1, Pallas kernels, fused_shards(): pl.pallas_call(functools.partial(fused_kernel, plan), out_shape=jax.Shape...  74.1 us
    unnamed x1, local copies, waits for them, and re-layouts  1.57 us

profile of v1, /device:TPU:0, one launch (start us, length us, event | category | flops | bytes accessed | tf_op | source)
XLA Modules:
  0.0 78.2 jit_solution(18102936010132990180)
XLA Ops:
  0.0 1.3 %broadcast_in_dim.18.gain_a = bf16[1,1024]{1,0:T(2,128)(2,1)} reshape(bf16[1024]{0:T(1024)(128)(2,1)} %param.12) | data formatting | bytes 4096 | tf_op jit(solution)/shard_map/broadcast_in_dim | solution.py:342
  1.3 1.3 %broadcast_in_dim.21.gain_b = bf16[1,1024]{1,0:T(2,128)(2,1)} reshape(bf16[1024]{0:T(1024)(128)(2,1)} %param.17) | data formatting | bytes 4096 | tf_op jit(solution)/shard_map/broadcast_in_dim | solution.py:345
  2.5 74.1 %shard_map.109 = bf16[64,1024]{1,0:T(8,128)(2,1)} custom-call(bf16[64,1024]{1,0:T(8,128)(2,1)} %tokens_ref.1, bf16[1,1024]{1,0:T(2,128)(2,1)} %broadcast_in_dim.18.gain_a, f32[1,4096]{1,0:T(1,128)} %bitcast.4, f32[1,1024]{1,0:T(1,128)} %bitcast.6, bf16[1,1024]{1,0:T(2,128)(2,1)} %broadcast_in_dim.21.gain_b, f32[1,4096]{1,0:T(1,128)} %bitcast.5, ...), custom_call_target="tpu_custom_call" | custom-call | tf_op jit(solution)/shard_map/pallas_call | solution.py:312
  76.7 1.6 %copy.13 = bf16[64,1024]{1,0:T(8,128)(2,1)} copy(bf16[64,1024]{1,0:T(8,128)(2,1)} %shard_map.109) | data formatting | bytes 262144

commit v2 on v1

--- a/solution.py
+++ b/solution.py
@@ -34,9 +34,10 @@
     out_ref,
     weights,
     scaled,
-    own_partial,
+    partial,
     rs_out,
     rs_in,
+    relay_in,
     stat_out,
     stat_in,
     hidden_own,
@@ -49,7 +50,9 @@
     w_sem,
     rs_sem,
     stat_sem,
+    relay_sem,
     ag_sem,
+    own_sem,
     cb_sem,
     cg_sem,
 ):
@@ -78,7 +81,7 @@
         return pltpu.make_async_copy(source.at[pl.ds(start, units), :], weights.at[buffer, j], w_sem.at[2 * layer + 1, j])
 
     up_order = ra_order + [0]
-    down_order = [0] + ra_order
+    down_order = [0] + sorted(ra_order, key=lambda j: min(j, n_ra - j))
     queue = [up_copy(0, j) for j in up_order] + [down_copy(0, j) for j in down_order]
     queue += [up_copy(1, j) for j in up_order]
     issued = [0]
@@ -100,20 +103,58 @@
     lane_ids = lax.broadcasted_iota(jnp.int32, (rows, LANES), 1)
     eye = row_ids == lane_ids
 
-    def send(axis, index, count, j, source, target, sem):
-        copy = pltpu.make_async_remote_copy(
+    def remote(axis, device, source, target, send_sem, recv_sem):
+        return pltpu.make_async_remote_copy(
             src_ref=source,
             dst_ref=target,
-            send_sem=sem.at[0],
-            recv_sem=sem.at[1],
-            device_id={axis: lax.rem(index + j, count)},
+            send_sem=send_sem,
+            recv_sem=recv_sem,
+            device_id={axis: device},
             device_id_type=MESH,
         )
+
+    def start_if(condition, copy):
+        pl.when(condition)(copy.start)
+        sends.append((condition, copy))
+        return copy
+
+    def send(axis, index, count, j, source, target, sem):
+        copy = remote(axis, lax.rem(index + j, count), source, target, sem.at[0], sem.at[1])
         copy.start()
-        sends.append(copy)
+        sends.append((None, copy))
         return copy
 
-    stat_copies, rs_copies, ag_copies, cb_copies, cg_copies = {}, {}, {}, {}, {}
+    first, last = r == 0, r == n_ra - 1
+    at_end = first | last
+    neighbour = jnp.where(first, 1, n_ra - 2)
+
+    def adds_relayed(j):
+        low = (r == 1) if j <= n_ra - 2 else False
+        high = (r == n_ra - 2) if j >= 2 else False
+        return low | high
+
+    def goes_direct(j):
+        inner = jnp.logical_not(at_end) & jnp.logical_not(adds_relayed(j))
+        if j == 1:
+            inner = inner | first
+        if j == n_ra - 1:
+            inner = inner | last
+        return inner
+
+    def goes_to_neighbour(j):
+        if j == 1:
+            return last
+        if j == n_ra - 1:
+            return first
+        return at_end
+
+    def arrives(j):
+        source = lax.rem(r + n_ra - j, n_ra)
+        from_first = (source == 0) & (r != 1)
+        from_last = (source == n_ra - 1) & (r != n_ra - 2)
+        return jnp.logical_not(from_first | from_last)
+
+    stat_copies, rs_copies, cb_copies, cg_copies = {}, {}, {}, {}
     waited = set()
 
     def span(g):
@@ -124,7 +165,7 @@
         squares = jnp.sum(values * values, axis=1, keepdims=True)
         as_row = jnp.sum(jnp.where(eye, squares, 0.0), axis=0, keepdims=True)
         stat_out[layer, g] = jnp.broadcast_to(as_row, (8, LANES))
-        scaled[layer, span(g), :] = (values * gains[layer][...].astype(jnp.float32)).astype(jnp.bfloat16)
+        scaled[layer, span(g), :] = (values * gains[layer][...].astype(jnp.float32).reshape(1, width)).astype(jnp.bfloat16)
 
     def send_stats(layer, g):
         for j in ra_order:
@@ -152,27 +193,39 @@
                     weights[buffer, j, :, columns].astype(jnp.bfloat16),
                     preferred_element_type=jnp.float32,
                 )
-                if j == 0:
-                    own_partial[pl.ds(low, count), columns] = value
-                else:
+                partial[j, pl.ds(low, count), columns] = value
+                if j:
                     rs_out[layer, j - 1, pl.ds(low, count), columns] = value.astype(jnp.bfloat16)
                 return carry
 
             lax.fori_loop(0, units // tile, body, 0)
             if j:
                 for g in members:
-                    rs_copies[layer, g, j] = send(
-                        "ra",
-                        r,
-                        n_ra,
-                        j,
-                        rs_out.at[layer, j - 1, span(g), :],
-                        rs_in.at[layer, j - 1, span(g), :],
-                        rs_sem.at[layer, g, j - 1],
-                    )
+                    source = rs_out.at[layer, j - 1, span(g), :]
+                    target = rs_in.at[layer, j - 1, span(g), :]
+                    sem = rs_sem.at[layer, g, j - 1]
+                    copy = remote("ra", lax.rem(r + j, n_ra), source, target, sem.at[0], sem.at[1])
+                    rs_copies[layer, g, j] = start_if(goes_direct(j), copy)
+                    place = jnp.where(first, max(j - 2, 0), min(j, n_ra - 2))
+                    target = relay_in.at[layer, place, span(g), :]
+                    sem = relay_sem.at[layer, g]
+                    copy = remote("ra", neighbour, source, target, sem.at[j - 1, 0], sem.at[place, 1])
+                    start_if(goes_to_neighbour(j), copy)
+
+    def relay_stage(layer, g):
+        for j in ra_order:
+
+            @pl.when(adds_relayed(j))
+            def _():
+                sem = relay_sem.at[layer, g, j - 1]
+                target = relay_in.at[layer, j - 1, span(g), :]
+                remote("ra", neighbour, target, target, sem.at[0], sem.at[1]).wait_recv()
+                added = partial[j, span(g), :] + target[...].astype(jnp.float32)
+                rs_out[layer, j - 1, span(g), :] = added.astype(jnp.bfloat16)
+
+            start_if(adds_relayed(j), rs_copies[layer, g, j])
 
     def reduce_stage(layer, g):
-        total = own_partial[span(g), :]
         squares = stat_out[layer, g]
         for j in ra_order:
             stat_copies[layer, g, j].wait_recv()
@@ -180,28 +233,49 @@
         as_column = jnp.sum(jnp.where(eye, jnp.broadcast_to(squares[0:1, :], (rows, LANES)), 0.0), axis=1, keepdims=True)
         inverse = lax.rsqrt(as_column / full_width + epsilon)
         for j in ra_order:
-            rs_copies[layer, g, j].wait_recv()
-            total = total + rs_in[layer, j - 1, span(g), :].astype(jnp.float32)
+
+            @pl.when(arrives(j))
+            def _():
+                rs_copies[layer, g, j].wait_recv()
+                partial[0, span(g), :] += rs_in[layer, j - 1, span(g), :].astype(jnp.float32)
+
+        total = partial[0, span(g), :]
         scale = up_scales[layer][:, pl.ds(pl.multiple_of(r * units, LANES), units)]
         active = jnp.square(jnp.maximum(total * inverse * scale, 0.0))
         hidden_own[layer, span(g), :] = active.astype(jnp.bfloat16)
-        for j in ra_order:
-            ag_copies[layer, g, j] = send(
-                "ra",
-                r,
-                n_ra,
-                j,
-                hidden_own.at[layer, span(g), :],
-                hidden_in.at[layer, j - 1, span(g), :],
-                ag_sem.at[layer, g, j - 1],
-            )
+        source = hidden_own.at[layer, span(g), :]
+        sem = ag_sem.at[layer, g]
+        right = remote("ra", lax.rem(r + 1, n_ra), source, hidden_in.at[layer, 0, span(g), :], own_sem.at[layer, g, 0], sem.at[0, 1])
+        left = remote(
+            "ra",
+            lax.rem(r + n_ra - 1, n_ra),
+            source,
+            hidden_in.at[layer, n_ra - 2, span(g), :],
+            own_sem.at[layer, g, 1],
+            sem.at[n_ra - 2, 1],
+        )
+        start_if(jnp.logical_not(last), right)
+        start_if(jnp.logical_not(first), left)
+
+    def take_hidden(layer, g, j):
+        sem = ag_sem.at[layer, g]
+        source = hidden_in.at[layer, j - 1, span(g), :]
+        remote("ra", lax.rem(r + 1, n_ra), source, source, sem.at[j - 1, 0], sem.at[j - 1, 1]).wait_recv()
+        if j < n_ra - 1:
+            target = hidden_in.at[layer, j, span(g), :]
+            copy = remote("ra", lax.rem(r + 1, n_ra), source, target, sem.at[j - 1, 0], sem.at[j, 1])
+            start_if((r >= j) & jnp.logical_not(last), copy)
+        if j > 1:
+            target = hidden_in.at[layer, j - 2, span(g), :]
+            copy = remote("ra", lax.rem(r + n_ra - 1, n_ra), source, target, sem.at[j - 1, 0], sem.at[j - 2, 1])
+            start_if((r < j) & jnp.logical_not(first), copy)
 
     def down_stage(layer, g):
         buffer = (1, 0)[layer]
         for j in down_order:
             wait_weight("down", layer, j)
             if j:
-                ag_copies[layer, g, j].wait_recv()
+                take_hidden(layer, g, j)
 
             def body(i, carry):
                 columns = pl.ds(pl.multiple_of(i * tile, LANES), tile)
@@ -272,16 +346,24 @@
     for j in down_order:
         down_copy(1, j).start()
     for layer in range(2):
+        if layer == 0:
+            for g in everyone:
+                relay_stage(layer, g)
+        for stage in (reduce_stage, down_stage, combine_stage):
+            for g in everyone:
+                stage(layer, g)
         for g in everyone:
-            reduce_stage(layer, g)
-        for g in everyone:
-            down_stage(layer, g)
-            if g:
-                gather_stage(layer, g - 1)
-            combine_stage(layer, g)
-        gather_stage(layer, groups - 1)
-    for copy in sends:
-        copy.wait_send()
+            gather_stage(layer, g)
+            if layer == 0:
+                if g:
+                    relay_stage(1, g - 1)
+                if g == groups - 1:
+                    relay_stage(1, g)
+    for condition, copy in sends:
+        if condition is None:
+            copy.wait_send()
+        else:
+            pl.when(condition)(copy.wait_send)
 
 
 def fused_shards(
@@ -317,7 +399,8 @@
         scratch_shapes=[
             pltpu.VMEM((3, n_ra, width, units), f32),
             pltpu.VMEM((2, rows_all, width), bf),
-            pltpu.VMEM((rows_all, units), f32),
+            pltpu.VMEM((n_ra, rows_all, units), f32),
+            pltpu.VMEM((2, n_ra - 1, rows_all, units), bf),
             pltpu.VMEM((2, n_ra - 1, rows_all, units), bf),
             pltpu.VMEM((2, n_ra - 1, rows_all, units), bf),
             pltpu.VMEM((2, groups, 8, LANES), f32),
@@ -333,16 +416,18 @@
             sems(n_ra),
             sems(n_ra),
             sems(n_ra),
+            sems(n_ra),
+            pltpu.SemaphoreType.DMA((2, groups, 2)),
             sems(n_cb),
             sems(n_cb),
         ],
         compiler_params=pltpu.CompilerParams(collective_id=0, has_side_effects=True, vmem_limit_bytes=VMEM_BYTES),
     )(
         tokens,
-        gain_first[None, :],
+        gain_first,
         up_scale_first[None, :],
         down_scale_first[None, :],
-        gain_second[None, :],
+        gain_second,
         up_scale_second[None, :],
         down_scale_second[None, :],
         up_first,
@@ -355,7 +440,7 @@
 def plan_for(mesh, d, ff, tokens):
     n_ra, n_cb, n_dp = mesh.shape["ra"], mesh.shape["cb"], mesh.shape["dp"]
     width, units, rows = d // n_ra, ff // (n_cb * n_ra), tokens // n_dp
-    if n_ra < 2 or n_cb < 2 or width != units or width % (n_cb * LANES) or rows % 16 or rows > LANES:
+    if n_ra < 4 or n_cb < 2 or width != units or width % (n_cb * LANES) or rows % 16 or rows > LANES:
         return None
     if 3 * n_ra * width * units * 4 > VMEM_BYTES * 4 // 5:
         return None

time: 78.4 us -> 80.2 us (1.023)
  Pallas kernels: 74.1 us -> 78.5 us
  local copies, waits for them, and re-layouts: 4.12 us -> 1.57 us
    pallas_call x1, Pallas kernels: 74.1 us -> 78.5 us  [fused_shards(): pl.pallas_call(functools.partial(fused_kernel, plan), out_shape=jax.Shape...]
    broadcast_in_dim x2 -> x0, local copies, waits for them, and re-layouts: 2.55 us -> none  [the longest x1 1.28 us: fused_shards(): gain_first[None, :]]
where the time goes in v2:
time: 80.2 us; the launch traced here: 80.1 us
  Pallas kernels  78.5 us (98%)
  local copies, waits for them, and re-layouts  1.57 us (2%)
    pallas_call x1, Pallas kernels, fused_shards(): pl.pallas_call(functools.partial(fused_kernel, plan), out_shape=jax.Shape...  78.5 us

profile of v2, /device:TPU:0, one launch (start us, length us, event | category | flops | bytes accessed | tf_op | source)
XLA Modules:
  0.0 80.1 jit_solution(14817066591509595981)
XLA Ops:
  0.0 78.5 %shard_map.109 = bf16[64,1024]{1,0:T(8,128)(2,1)} custom-call(bf16[64,1024]{1,0:T(8,128)(2,1)} %tokens_ref.1, bf16[1024]{0:T(1024)(128)(2,1)} %gain_a.1, f32[1,4096]{1,0:T(1,128)} %bitcast.4, f32[1,1024]{1,0:T(1,128)} %bitcast.6, bf16[1024]{0:T(1024)(128)(2,1)} %gain_b.1, f32[1,4096]{1,0:T(1,128)} %bitcast.5, f32[1,1024]{1,0:T(1,128)} %bitcast.7, ...), custom_call_target="tpu_custom_call" | custom-call | tf_op jit(solution)/shard_map/pallas_call | solution.py:394
  78.5 1.6 %copy.13 = bf16[64,1024]{1,0:T(8,128)(2,1)} copy(bf16[64,1024]{1,0:T(8,128)(2,1)} %shard_map.109) | data formatting | bytes 262144
